TPU v7x, 32 devices: a whole 2x2x4 slice. The times are simulated.
32 devices in a mesh: grp: 2 (over x), ep: 16 (over z, y, core).
Axes of the slice: x: 2, y: 2, z: 4, core: 2. Of those that a mesh axis runs over, the one named last changes fastest.
Arguments:
- tokens: bfloat16 [384, 2048], P(('grp', 'ep')), parts along dimension 0, may hold values from -6 to 6
- norm_gain: float32 [2048], replicated, may hold values from 0.1 to 1.9
- query_weight: bfloat16 [2048, 512], P('ep'), may hold values from -0.125 to 0.125
- key_weight: bfloat16 [2048, 512], P('ep'), may hold values from -0.125 to 0.125
- value_weight: bfloat16 [2048, 512], P('ep'), may hold values from -0.125 to 0.125
- outgate_weight: bfloat16 [2048, 512], P('ep'), may hold values from -0.125 to 0.125
- ingate_weight: bfloat16 [2048, 4], P('ep'), may hold values from -0.125 to 0.125
- forget_weight: bfloat16 [2048, 4], P('ep'), may hold values from -0.125 to 0.125
- ingate_bias: float32 [4], replicated, may hold values from -1 to 1
- forget_bias: float32 [4], replicated, may hold values from 0.5 to 4
- memory: float32 [384, 4, 128, 128], P(('grp', 'ep')), parts along dimension 0, may hold values from -4 to 4
- normalizer: float32 [384, 4, 128], P(('grp', 'ep')), parts along dimension 0, may hold values from -4 to 4
- stabilizer: float32 [384, 4], P(('grp', 'ep')), parts along dimension 0, may hold values from -1 to 2
- mixer_weight: bfloat16 [512, 2048], P(None, 'ep'), may hold values from -0.25 to 0.25
- moe_gain: float32 [2048], replicated, may hold values from 0.1 to 1.9
- expert_gate: bfloat16 [16, 2048, 512], P('ep'), may hold values from -0.125 to 0.125
- expert_up: bfloat16 [16, 2048, 512], P('ep'), may hold values from -0.125 to 0.125
- expert_down: bfloat16 [16, 512, 2048], P('ep'), may hold values from -0.25 to 0.25
- expert_index: int32 [384, 6], P(('grp', 'ep')), parts along dimension 0, may hold values from 0 to 15, as said below
- route_weights: float32 [384, 6], P(('grp', 'ep')), parts along dimension 0, may hold values from 0.1 to 1
Outputs:
- layer_out: bfloat16 [384, 2048], P(('grp', 'ep')), parts along dimension 0
- new_memory: float32 [384, 4, 128, 128], P(('grp', 'ep')), parts along dimension 0
- new_normalizer: float32 [384, 4, 128], P(('grp', 'ep')), parts along dimension 0
- new_stabilizer: float32 [384, 4], P(('grp', 'ep')), parts along dimension 0
There are 2 independent parts, one for each index of `grp`. A program takes and returns all parts, laid end to end along the dimension named above; an argument that names none is the same for every part. Nothing has to cross between parts.
Inputs may be any that keep to these rules, and one draw needn't show every extreme that they name: `expert_index`: experts 0 to 15 form two groups of 8 consecutive numbers; each row names 6 different experts of one group. Among the 12 rows of one device at most 5 name one expert, and in every device some expert is named by exactly 5 of them.
All inputs are finite; a program needn't handle non-finite values.
Results may differ from a plain program's by a relative error of at most 0.013.
Values may be sent and summed in bfloat16 or wider, within the bound.
A program may use at most 128 MiB of HBM per device.

v0:
```python
import jax
import jax.numpy as jnp
from jax import lax
from jax.sharding import PartitionSpec as P

M_HEAD_DIM = 128


EPS = 1e-06


def rms_normed(values, gain):
    scale = lax.rsqrt(jnp.mean(values * values, axis=-1, keepdims=True) + EPS)
    return values * scale * gain


def on_device(
    tokens,
    norm_gain,
    query_weight,
    key_weight,
    value_weight,
    outgate_weight,
    ingate_weight,
    forget_weight,
    ingate_bias,
    forget_bias,
    memory,
    normalizer,
    stabilizer,
    mixer_weight,
    moe_gain,
    expert_gate,
    expert_up,
    expert_down,
    expert_index,
    route_weights,
):
    f32 = jnp.float32
    bf16 = jnp.bfloat16
    ep_size = lax.axis_size("ep")
    seq_count = tokens.shape[0]
    model_width = tokens.shape[1]
    cell_width = query_weight.shape[1]
    head_count = ingate_bias.shape[0]
    stream = tokens.astype(f32)
    weight_list = (
        query_weight,
        key_weight,
        value_weight,
        outgate_weight,
        ingate_weight,
        forget_weight,
    )
    normed = rms_normed(stream, norm_gain).astype(bf16)
    normed_cols = lax.all_to_all(normed, "ep", split_axis=1, concat_axis=0, tiled=True)
    joined = jnp.concatenate(weight_list, axis=1)
    projected = lax.psum_scatter(
        jnp.dot(normed_cols, joined, preferred_element_type=f32),
        "ep",
        scatter_dimension=0,
        tiled=True,
    )
    query_sum = projected[:, :cell_width]
    key_sum = projected[:, cell_width : 2 * cell_width]
    value_sum = projected[:, 2 * cell_width : 3 * cell_width]
    outgate_sum = projected[:, 3 * cell_width : 4 * cell_width]
    ingate_sum = projected[:, 4 * cell_width : 4 * cell_width + head_count]
    forget_sum = projected[:, 4 * cell_width + head_count :]
    shape = (seq_count, head_count, M_HEAD_DIM)
    query_heads = query_sum.astype(bf16).astype(f32).reshape(shape)
    key_heads = key_sum.astype(bf16).astype(f32).reshape(shape) * M_HEAD_DIM ** (-0.5)
    value_heads = value_sum.astype(bf16).astype(f32).reshape(shape)
    outgate = outgate_sum.astype(bf16).astype(f32)
    ingate_pre = ingate_sum + ingate_bias
    forget_pre = forget_sum + forget_bias
    log_forget = jax.nn.log_sigmoid(forget_pre)
    new_stabilizer = jnp.maximum(log_forget + stabilizer, ingate_pre)
    keep = jnp.exp(log_forget + stabilizer - new_stabilizer)
    write = jnp.exp(ingate_pre - new_stabilizer)
    new_memory = (
        keep[..., None, None] * memory
        + write[..., None, None] * key_heads[..., :, None] * value_heads[..., None, :]
    )
    new_normalizer = keep[..., None] * normalizer + write[..., None] * key_heads
    numer = jnp.einsum("thd,thde->the", query_heads, new_memory, precision=lax.Precision.HIGHEST)
    denom = jnp.sum(query_heads * new_normalizer, axis=-1)
    hidden = numer / jnp.maximum(jnp.abs(denom), 1.0)[..., None]
    cell_out = (hidden.reshape(seq_count, cell_width) * jax.nn.sigmoid(outgate)).astype(bf16)
    mixed_cols = jnp.dot(
        lax.all_gather(cell_out, "ep", axis=0, tiled=True), mixer_weight, preferred_element_type=f32
    ).astype(bf16)
    mixed = lax.all_to_all(mixed_cols, "ep", split_axis=0, concat_axis=1, tiled=True)
    resid = stream + mixed.astype(f32)
    moe_in = rms_normed(resid, moe_gain).astype(bf16)
    local_experts = expert_gate.shape[0]
    expert_count = local_experts * ep_size
    chosen_k = expert_index.shape[1]
    group_width = expert_count // 2
    capacity = max(2, ((seq_count + 1) // 2 * chosen_k + group_width - 1) // group_width)
    routes = expert_index.reshape(-1)
    matches = (routes[:, None] == jnp.arange(expert_count, dtype=jnp.int32)[None, :]).astype(
        jnp.int32
    )
    slots = jnp.sum((jnp.cumsum(matches, axis=0) - 1) * matches, axis=1)
    target = routes * capacity + slots
    placing = (
        jnp.arange(expert_count * capacity, dtype=jnp.int32)[:, None] == target[None, :]
    ).astype(bf16)
    route_rows = jnp.repeat(moe_in, chosen_k, axis=0)
    outgoing = jnp.dot(placing, route_rows, preferred_element_type=f32).astype(bf16)
    outgoing = outgoing.reshape(expert_count, capacity, model_width)
    received = lax.all_to_all(outgoing, "ep", split_axis=0, concat_axis=0, tiled=True)
    count = received.shape[1]
    grouped = received.reshape(ep_size, local_experts, count, model_width)
    gate = jnp.einsum("sxcd,xdf->sxcf", grouped, expert_gate, preferred_element_type=f32)
    upward = jnp.einsum("sxcd,xdf->sxcf", grouped, expert_up, preferred_element_type=f32)
    inner = (jax.nn.silu(gate) * upward).astype(bf16)
    result = jnp.einsum("sxcf,xfd->sxcd", inner, expert_down, preferred_element_type=f32).astype(
        bf16
    )
    result = result.reshape(ep_size * local_experts, count, model_width)
    returned = lax.all_to_all(result, "ep", split_axis=0, concat_axis=0, tiled=True)
    flat_back = returned.reshape(expert_count * capacity, model_width)
    picked = jnp.dot(placing.T, flat_back, preferred_element_type=f32)
    weighted = picked * route_weights.reshape(-1)[:, None]
    combined = jnp.sum(weighted.reshape(seq_count, chosen_k, model_width), axis=1)
    layer_out = (resid + combined).astype(bf16)
    return (layer_out, new_memory, new_normalizer, new_stabilizer)


def solution(mesh):
    return jax.shard_map(
        on_device,
        mesh=mesh,
        in_specs=(
            P(("grp", "ep"), None),
            P(),
            P("ep", None),
            P("ep", None),
            P("ep", None),
            P("ep", None),
            P("ep", None),
            P("ep", None),
            P(),
            P(),
            P(("grp", "ep"), None, None, None),
            P(("grp", "ep"), None, None),
            P(("grp", "ep"), None),
            P(None, "ep"),
            P(),
            P("ep", None, None),
            P("ep", None, None),
            P("ep", None, None),
            P(("grp", "ep"), None),
            P(("grp", "ep"), None),
        ),
        out_specs=(
            P(("grp", "ep"), None),
            P(("grp", "ep"), None, None, None),
            P(("grp", "ep"), None, None),
            P(("grp", "ep"), None),
        ),
        check_vma=False,
    )
```

profile of v0, /device:TPU:0, one launch (start us, length us, event | category | flops | bytes accessed | tf_op | source)
XLA Modules:
  0.0 214.0 jit_solution(910980491938122106)
XLA Ops:
  7.2 1.1 fusion.30
  8.3 0.9 fusion.32
  9.9 7.4 %all-to-all-start = ((bf16[12,16,128]{2,0,1:T(8,128)(2,1)}), bf16[12,16,128]{2,0,1:T(8,128)(2,1)S(1)}, u32[]{:S(2)}, u32[]{:S(2)}) async-start(bf16[12,16,128]{2,0,1:T(8,128)(2,1)} %copy.51), calls=%async_computation | async-start | bytes 131072 | tf_op jit(solution)/shard_map/all_to_all | solution.py:56
  19.0 1.2 concatenate.3
  20.2 4.0 %all-to-all-done = bf16[12,16,128]{2,0,1:T(8,128)(2,1)S(1)} async-done(((bf16[12,16,128]{2,0,1:T(8,128)(2,1)}), bf16[12,16,128]{2,0,1:T(8,128)(2,1)S(1)}, u32[]{:S(2)}, u32[]{:S(2)}) %all-to-all-start) | async-done | bytes 49184 | tf_op jit(solution)/shard_map/all_to_all | solution.py:56
  24.3 1.5 fusion.44
  27.8 92.5 %all-reduce.3.cloned.1.call-done = f32[192,2056]{1,0:T(8,128)} async-done(((f32[192,2056]{1,0:T(8,128)}), f32[192,2056]{1,0:T(8,128)}) %all-reduce.3.cloned.1.call-update) | async-done | bytes 1579024
  120.2 0.9 dynamic-slice_convert_fusion
  121.3 0.9 subtract_exponential_fusion
  123.7 2.5 %multiply_add_fusion = f32[12,4,128,128]{3,2,1,0:T(8,128)S(1)} fusion(f32[12,4,128,128]{3,2,1,0:T(8,128)} %param.30, f32[12,4,128]{2,1,0:T(4,128)S(1)} %reshape.131, f32[12,4,128]{2,1,0:T(4,128)S(1)} %get-tuple-element.22, f32[12,4]{1,0:T(8,128)S(1)} %get-tuple-element.23), kind=kLoop, calls=%fused_computation | loop fusion | flops 2359296 | bytes 6340800 | tf_op jit(solution)/shard_map/add | solution.py:82
  126.2 1.7 copy-done.1
  127.8 1.5 fusion.45
  129.5 20.0 %all-gather = bf16[16,12,512]{2,1,0:T(8,128)(2,1)S(1)} all-gather(bf16[1,12,512]{2,1,0:T(8,128)(2,1)S(1)} %fusion.37), channel_id=1, replica_groups=mesh['grp'=2,'ep'=16] {'ep'}, dimensions={0}, use_global_device_ids=true | all-gather | bytes 208896 | tf_op jit(solution)/shard_map/all_gather | solution.py:91
  150.5 3.5 %all-to-all-start.1 = ((bf16[16,12,128]{2,1,0:T(8,128)(2,1)}), bf16[16,12,128]{2,1,0:T(8,128)(2,1)S(1)}, u32[]{:S(2)}, u32[]{:S(2)}) async-start(bf16[16,12,128]{2,1,0:T(8,128)(2,1)} %all_to_all.34), calls=%async_computation.1 | async-start | bytes 131072 | tf_op jit(solution)/shard_map/all_to_all | solution.py:93
  154.0 6.8 %all-to-all-done.1 = bf16[16,12,128]{2,1,0:T(8,128)(2,1)S(1)} async-done(((bf16[16,12,128]{2,1,0:T(8,128)(2,1)}), bf16[16,12,128]{2,1,0:T(8,128)(2,1)S(1)}, u32[]{:S(2)}, u32[]{:S(2)}) %all-to-all-start.1) | async-done | bytes 49184 | tf_op jit(solution)/shard_map/all_to_all | solution.py:93
  162.2 16.9 %all_to_all.42 = bf16[16,5,2048]{2,1,0:T(8,128)(2,1)S(1)} all-to-all(bf16[16,5,2048]{2,1,0:T(8,128)(2,1)S(1)} %reshape.122), channel_id=1, replica_groups=mesh['grp'=2,'ep'=16] {'ep'}, dimensions={0} | all-to-all | bytes 655360 | tf_op jit(solution)/shard_map/all_to_all | solution.py:113
  179.1 2.1 fusion.5
  181.3 2.6 %convolution_convert_fusion = bf16[16,5,2048]{2,0,1:T(8,128)(2,1)S(1)} fusion(bf16[1,512,2048]{2,1,0:T(8,128)(2,1)S(1)} %copy-done, bf16[1,2048,512]{2,1,0:T(8,128)(2,1)} %param.36, bf16[16,5,2048]{2,1,0:T(8,128)(2,1)S(1)} %all_to_all.42, f32[16,1,5,512]{3,0,2,1:T(8,128)S(1)} %fusion.5), kind=kOutput, calls=%fused_computation.2 | convolution fusion | flops 335953920 | bytes 5013504 | tf_op jit(solution)/shard_map/sxcf,xfd->sxcd/dot_general | solution.py:119
  183.8 1.0 copy.59
  184.8 4.1 %all-to-all-start.3 = ((bf16[16,5,2048]{2,1,0:T(8,128)(2,1)}), bf16[16,5,2048]{2,1,0:T(8,128)(2,1)S(1)}, u32[]{:S(2)}, u32[]{:S(2)}) async-start(bf16[16,5,2048]{2,1,0:T(8,128)(2,1)} %copy.59), calls=%async_computation.3 | async-start | bytes 1048576 | tf_op jit(solution)/shard_map/all_to_all | solution.py:123
  189.8 13.4 %all-to-all-done.3 = bf16[16,5,2048]{2,1,0:T(8,128)(2,1)S(1)} async-done(((bf16[16,5,2048]{2,1,0:T(8,128)(2,1)}), bf16[16,5,2048]{2,1,0:T(8,128)(2,1)S(1)}, u32[]{:S(2)}, u32[]{:S(2)}) %all-to-all-start.3) | async-done | bytes 327712 | tf_op jit(solution)/shard_map/all_to_all | solution.py:123
  203.2 0.9 reshape.127
  204.1 1.3 convolution_multiply_fusion
  205.6 1.6 add_convert_fusion
  (73 shorter events, 8.7 us)
Async XLA Ops:
  7.2 174.1 %copy-start = (bf16[1,512,2048]{2,1,0:T(8,128)(2,1)S(1)}, bf16[1,512,2048]{2,1,0:T(8,128)(2,1)}, u32[]{:S(2)}) copy-start(bf16[1,512,2048]{2,1,0:T(8,128)(2,1)} %param.37) | copy-start | bytes 6291460
  9.9 14.3 %all-to-all-start = ((bf16[12,16,128]{2,0,1:T(8,128)(2,1)}), bf16[12,16,128]{2,0,1:T(8,128)(2,1)S(1)}, u32[]{:S(2)}, u32[]{:S(2)}) async-start(bf16[12,16,128]{2,0,1:T(8,128)(2,1)} %copy.51), calls=%async_computation | async-start | bytes 131072 | tf_op jit(solution)/shard_map/all_to_all | solution.py:56
  17.3 102.9 %all-reduce.3.cloned.1.call-start = ((), (), s32[]{:S(2)}) async-start(), calls=%async_computation.4 | async-start | bytes 3342336
  20.2 5.7 %copy-start.10 = (f32[12,4]{0,1:T(4,128)S(1)}, f32[12,4]{0,1:T(4,128)}, u32[]{:S(2)}) copy-start(f32[12,4]{0,1:T(4,128)} %param.32) | copy-start | bytes 580
  20.2 5.8 %copy-start.7 = (s32[12,6]{0,1:T(8,128)S(1)}, s32[12,6]{0,1:T(8,128)}, u32[]{:S(2)}) copy-start(s32[12,6]{0,1:T(8,128)} %param.38) | copy-start | bytes 868
  20.2 5.9 %copy-start.12 = (u32[32]{0:T(128)S(1)}, u32[32]{0:T(128)}, u32[]{:S(2)}) copy-start(u32[32]{0:T(128)} %constant.40) | copy-start | bytes 388
  24.3 97.0 %copy-start.9 = (f32[4]{0:T(128)S(1)}, f32[4]{0:T(128)}, u32[]{:S(2)}) copy-start(f32[4]{0:T(128)} %param.28) | copy-start | bytes 52
  24.3 97.0 %copy-start.11 = (f32[4]{0:T(128)S(1)}, f32[4]{0:T(128)}, u32[]{:S(2)}) copy-start(f32[4]{0:T(128)} %param.29) | copy-start | bytes 52
  24.3 98.7 %copy-start.5 = (f32[12,4,128]{2,1,0:T(4,128)S(1)}, f32[12,4,128]{2,1,0:T(4,128)}, u32[]{:S(2)}) copy-start(f32[12,4,128]{2,1,0:T(4,128)} %param.31) | copy-start | bytes 73732
  126.2 1.7 copy-start.1
  127.8 21.8 %copy-start.4 = (bf16[512,128]{1,0:T(8,128)(2,1)S(1)}, bf16[512,128]{1,0:T(8,128)(2,1)}, u32[]{:S(2)}) copy-start(bf16[512,128]{1,0:T(8,128)(2,1)} %param.33) | copy-start | bytes 393220
  127.8 33.1 %copy-start.3 = (bf16[12,2048]{1,0:T(8,128)(2,1)S(1)}, bf16[12,2048]{1,0:T(8,128)(2,1)}, u32[]{:S(2)}) copy-start(bf16[12,2048]{1,0:T(8,128)(2,1)} %param.20) | copy-start | bytes 147460
  129.4 32.2 %copy-start.6 = (f32[2048]{0:T(1024)S(1)}, f32[2048]{0:T(1024)}, u32[]{:S(2)}) copy-start(f32[2048]{0:T(1024)} %param.34) | copy-start | bytes 24580
  150.5 10.4 %all-to-all-start.1 = ((bf16[16,12,128]{2,1,0:T(8,128)(2,1)}), bf16[16,12,128]{2,1,0:T(8,128)(2,1)S(1)}, u32[]{:S(2)}, u32[]{:S(2)}) async-start(bf16[16,12,128]{2,1,0:T(8,128)(2,1)} %all_to_all.34), calls=%async_computation.1 | async-start | bytes 131072 | tf_op jit(solution)/shard_map/all_to_all | solution.py:93
  161.0 0.6 copy-start.2
  181.3 7.7 %copy-start.8 = (f32[12,6]{0,1:T(8,128)S(1)}, f32[12,6]{0,1:T(8,128)}, u32[]{:S(2)}) copy-start(f32[12,6]{0,1:T(8,128)} %param.39) | copy-start | bytes 868
  184.8 18.4 %all-to-all-start.3 = ((bf16[16,5,2048]{2,1,0:T(8,128)(2,1)}), bf16[16,5,2048]{2,1,0:T(8,128)(2,1)S(1)}, u32[]{:S(2)}, u32[]{:S(2)}) async-start(bf16[16,5,2048]{2,1,0:T(8,128)(2,1)} %copy.59), calls=%async_computation.3 | async-start | bytes 1048576 | tf_op jit(solution)/shard_map/all_to_all | solution.py:123
Sparse Core Ops, SparseCore 0:
  26.0 94.2 all-reduce.2
where the time goes:
time: 215 us; the launch traced here: 214 us
  waiting for transfers between devices  117 us (54%)
  blocking collectives  36.9 us (17%)
  starting transfers between devices  15.1 us (7%)
  between operations  15.1 us (7%)
  local copies, waits for them, and re-layouts  11.4 us (5%)
  other arithmetic  9.43 us (4%)
  matrix products  9.42 us (4%)
    unnamed x2, waiting for transfers between devices  92.5 us
    all_gather x1, blocking collectives, on_device(): lax.all_gather(cell_out, 'ep', axis=0, tiled=True)  20 us
    all_to_all x1, blocking collectives, on_device(): lax.all_to_all(outgoing, 'ep', split_axis=0, concat_axis=0, tiled=True)  16.9 us
    all_to_all x1, waiting for transfers between devices, on_device(): lax.all_to_all(result, 'ep', split_axis=0, concat_axis=0, tiled=True)  13.4 us
    all_to_all x1, starting transfers between devices, on_device(): lax.all_to_all(normed, 'ep', split_axis=1, concat_axis=0, tiled=True)  7.41 us
    all_to_all x1, waiting for transfers between devices, on_device(): lax.all_to_all(mixed_cols, 'ep', split_axis=0, concat_axis=1, tiled=True)  6.85 us
    unnamed x39, local copies, waits for them, and re-layouts  5.48 us
  transfers between devices with their start and end apart: 4, of which 4 were waited for; matrix products, arithmetic and copies ran while one was open for 2% of the time, Pallas kernels for 0%

commit v1 on v0

v1 whole, which is shorter than its diff:
```python
import functools

import jax
import jax.numpy as jnp
from jax import lax
from jax.experimental import pallas as pl
from jax.experimental.pallas import tpu as pltpu
from jax.sharding import PartitionSpec as P

M_HEAD_DIM = 128
LANES = 128
HALF = 64
EPS = 1e-06
f32 = jnp.float32
bf16 = jnp.bfloat16


def rms_normed(values, gain):
    scale = lax.rsqrt(jnp.mean(values * values, axis=-1, keepdims=True) + EPS)
    return values * scale * gain


def remote(src, dst, send_sem, recv_sem, device):
    return pltpu.make_async_remote_copy(
        src_ref=src,
        dst_ref=dst,
        send_sem=send_sem,
        recv_sem=recv_sem,
        device_id={"ep": device},
        device_id_type=pl.DeviceIdType.MESH,
    )


def loop(low, high, body):
    def step(index, carry):
        body(index)
        return carry

    lax.fori_loop(low, high, step, 0)


def split_lanes(values):
    lane = lax.broadcasted_iota(jnp.int32, values.shape, 1)
    high = values.astype(bf16).astype(f32)
    return jnp.where(lane < HALF, high, values - high).astype(bf16)


def layer_kernel(
    n,
    seq,
    group_width,
    tokens,
    norm_gain,
    ingate_weight,
    forget_weight,
    ingate_bias,
    forget_bias,
    normalizer,
    stabilizer,
    moe_gain,
    expert_index,
    route_weights,
    query_weight,
    key_weight,
    value_weight,
    outgate_weight,
    memory,
    mixer_weight,
    expert_gate,
    expert_up,
    expert_down,
    layer_out,
    new_normalizer,
    new_stabilizer,
    new_memory,
    proj_w,
    gate_w,
    mem,
    mix_w,
    gate_e,
    up_e,
    down_e,
    normed,
    normed_cols,
    part,
    pair_send,
    pair_recv,
    sum_send,
    sum_recv,
    key_t,
    query_t,
    value_rows,
    keep_rows,
    numer,
    cells,
    mixed_send,
    mixed,
    resid_rows,
    packed,
    routed,
    outcome,
    back_pair_send,
    back_pair_recv,
    back_send,
    back_recv,
    load_sem,
    store_sem,
    send_a,
    recv_a,
    send_b,
    recv_b,
    send_c,
    recv_c,
    send_d,
    recv_d,
    send_e,
    recv_e,
    send_f,
    recv_f,
    send_g,
    recv_g,
    send_h,
    recv_h,
    send_i,
    recv_i,
):
    me = lax.axis_index("ep")
    core = lax.rem(me, 2)
    chip = me // 2
    partner = me + 1 - 2 * core
    chips = n // 2
    width = proj_w.shape[1] // 4
    heads = mem.shape[1]
    model = tokens.shape[1]
    slots = packed.shape[1]

    loads = [
        pltpu.make_async_copy(source, target, load_sem.at[index])
        for index, (source, target) in enumerate(
            (
                (query_weight, proj_w.at[:, pl.ds(0, width)]),
                (key_weight, proj_w.at[:, pl.ds(width, width)]),
                (value_weight, proj_w.at[:, pl.ds(2 * width, width)]),
                (outgate_weight, proj_w.at[:, pl.ds(3 * width, width)]),
                (memory, mem),
                (mixer_weight, mix_w),
                (expert_gate, gate_e),
                (expert_up, up_e),
                (expert_down, down_e),
            )
        )
    ]
    for load in loads:
        load.start()

    barrier = pltpu.get_barrier_semaphore()

    def greet(k):
        pl.semaphore_signal(
            barrier,
            inc=1,
            device_id={"ep": lax.rem(me + k, n)},
            device_id_type=pl.DeviceIdType.MESH,
        )

    loop(1, n, greet)

    stream = tokens[...].astype(f32)
    depth = normed_cols.shape[2]
    scaled = rms_normed(stream, norm_gain[...]).astype(bf16)
    normed[:, pl.ds(seq, 16 - seq), :] = jnp.zeros((n, 16 - seq, depth), bf16)
    for d in range(n):
        normed[d, pl.ds(0, seq), :] = scaled[:, d * depth : (d + 1) * depth]
    gate_w[...] = jnp.zeros(gate_w.shape, bf16)
    for base in (0, HALF):
        gate_w[:, base : base + heads] = ingate_weight[...]
        gate_w[:, base + heads : base + 2 * heads] = forget_weight[...]

    pl.semaphore_wait(barrier, n - 1)

    def send_cols(k):
        to = lax.rem(me + k, n)
        remote(normed.at[to], normed_cols.at[me], send_a.at[to], recv_a.at[me], to).start()

    def wait_cols(k):
        of = lax.rem(me + k, n)
        remote(normed.at[of], normed_cols.at[of], send_a.at[of], recv_a.at[of], of).wait()

    loop(1, n, send_cols)
    normed_cols[me] = normed[me]
    for load in loads[:4]:
        load.wait()
    loop(1, n, wait_cols)

    rows = normed_cols[...].reshape(n * 16, depth)
    for piece in range(4):
        columns = slice(piece * width, (piece + 1) * width)
        block = jnp.dot(rows, proj_w[:, columns], preferred_element_type=f32)
        part[:, :, columns] = block.reshape(n, 16, width)
    gates = jnp.dot(rows, gate_w[...], preferred_element_type=f32)
    part[:, :, 4 * width :] = gates.reshape(n, 16, LANES)

    def pack_sums(values):
        return values[:, : 4 * width].astype(bf16), split_lanes(values[:, 4 * width :])

    def unpack_sums(values):
        narrow = values[:, 4 * width :]
        whole = narrow + pltpu.roll(narrow, HALF, 1)
        return jnp.concatenate([values[:, : 4 * width], whole], axis=1)

    def pair_copy(j):
        return remote(
            pair_send.at[j], pair_recv.at[j], send_b.at[j], recv_b.at[j], partner
        )

    def send_pair(k):
        j = lax.rem(chip + k, chips)
        wide, narrow = pack_sums(part[2 * j + 1 - core])
        pair_send[j, :, : 4 * width] = wide
        pair_send[j, :, 4 * width :] = narrow
        pair_copy(j).start()

    loop(1, chips + 1, send_pair)

    def sum_copy(j, slot):
        return remote(
            sum_send.at[j],
            sum_recv.at[slot],
            send_c.at[j],
            recv_c.at[slot],
            2 * j + core,
        )

    def send_sum(k):
        j = lax.rem(chip + k, chips)
        pair_copy(j).wait()
        wide, narrow = pack_sums(part[2 * j + core] + unpack_sums(pair_recv[j].astype(f32)))
        sum_send[j, :, : 4 * width] = wide
        sum_send[j, :, 4 * width :] = narrow
        sum_copy(j, chip).start()

    loop(1, chips, send_sum)
    pair_copy(chip).wait()
    own = part[me] + unpack_sums(pair_recv[chip].astype(f32))

    def wait_sum(k, total):
        j = lax.rem(chip + k, chips)
        sum_copy(j, j).wait()
        return total + sum_recv[j].astype(f32)

    others = lax.fori_loop(1, chips, wait_sum, jnp.zeros(own.shape, f32))
    sums = (own + unpack_sums(others))[:seq]

    scale = M_HEAD_DIM ** (-0.5)
    gates = sums[:, 4 * width : 4 * width + 2 * heads]
    ingate_pre = gates[:, :heads] + ingate_bias[...]
    forget_pre = gates[:, heads:] + forget_bias[...]
    log_forget = jnp.minimum(forget_pre, 0.0) - jnp.log1p(jnp.exp(-jnp.abs(forget_pre)))
    stable = jnp.maximum(log_forget + stabilizer[...], ingate_pre)
    new_stabilizer[...] = stable
    keep = jnp.exp(log_forget + stabilizer[...] - stable)
    write = jnp.exp(ingate_pre - stable)
    rank = (M_HEAD_DIM, M_HEAD_DIM)
    unit = (
        lax.broadcasted_iota(jnp.int32, rank, 0) == lax.broadcasted_iota(jnp.int32, rank, 1)
    ).astype(bf16)
    contract = (((1,), (1,)), ((), ()))
    denoms = []
    for h in range(heads):
        lanes = slice(h * M_HEAD_DIM, (h + 1) * M_HEAD_DIM)
        query = sums[:, 0 * width :][:, lanes].astype(bf16)
        key = sums[:, 1 * width :][:, lanes].astype(bf16)
        value = sums[:, 2 * width :][:, lanes].astype(bf16)
        query_t[h] = lax.dot_general(unit, query, contract, preferred_element_type=f32)
        key_t[h] = lax.dot_general(unit, key, contract, preferred_element_type=f32) * scale
        value_rows[h] = value.astype(f32) * write[:, h : h + 1]
        keep_rows[h] = jnp.broadcast_to(keep[:, h : h + 1], (seq, M_HEAD_DIM))
        fresh = (
            keep[:, h : h + 1] * normalizer[:, h, :]
            + write[:, h : h + 1] * key.astype(f32) * scale
        )
        new_normalizer[:, h, :] = fresh
        denoms.append(jnp.sum(query.astype(f32) * fresh, axis=-1, keepdims=True))
    loads[4].wait()

    def one_head(h):
        for t in range(seq):
            fresh = (
                keep_rows[h, t : t + 1, :] * mem[t, h]
                + key_t[h, :, t : t + 1] * value_rows[h, t : t + 1, :]
            )
            mem[t, h] = fresh
            numer[h, t : t + 1, :] = jnp.sum(
                query_t[h, :, t : t + 1] * fresh, axis=0, keepdims=True
            )

    loop(0, heads, one_head)
    memory_store = pltpu.make_async_copy(mem, new_memory, store_sem.at[0])
    memory_store.start()
    outgate = sums[:, 3 * width : 4 * width].astype(bf16).astype(f32)
    opened = jax.nn.sigmoid(outgate)
    cells[me] = jnp.zeros(cells.shape[1:], bf16)
    for h in range(heads):
        lanes = slice(h * M_HEAD_DIM, (h + 1) * M_HEAD_DIM)
        hidden = numer[h] / jnp.maximum(jnp.abs(denoms[h]), 1.0)
        cells[me, pl.ds(0, seq), lanes] = (hidden * opened[:, lanes]).astype(bf16)

    def cell_copy(to, slot):
        return remote(cells.at[slot], cells.at[slot], send_d.at[to], recv_d.at[slot], to)

    loop(1, n, lambda k: cell_copy(lax.rem(me + k, n), me).start())
    loads[5].wait()

    def wait_cell(k):
        of = lax.rem(me + k, n)
        cell_copy(of, of).wait_recv()

    loop(1, n, wait_cell)
    mixes = jnp.dot(
        cells[...].reshape(n * 16, width), mix_w[...], preferred_element_type=f32
    ).astype(bf16)
    mixed_send[...] = mixes.reshape(n, 16, depth)

    def mixed_copy(to, slot):
        return remote(mixed_send.at[to], mixed.at[slot], send_e.at[to], recv_e.at[slot], to)

    loop(1, n, lambda k: mixed_copy(lax.rem(me + k, n), me).start())
    mixed[me] = mixed_send[me]

    index = expert_index[...]
    group = (index[:, 0:1] >= group_width).astype(jnp.int32)
    lane = lax.broadcasted_iota(jnp.int32, (seq, LANES), 1)
    named = group * group_width + jnp.where(lane < HALF, lane, lane - HALF)
    inside = jnp.where(lane < HALF, lane, lane - HALF) < group_width
    shares = jnp.zeros((seq, LANES), f32)
    for k in range(index.shape[1]):
        hit = (index[:, k : k + 1] == named) & inside
        shares = shares + jnp.where(hit, route_weights[:, k : k + 1], 0.0)
    shares = split_lanes(shares)
    square = (seq, seq)
    earlier = (
        lax.broadcasted_iota(jnp.int32, square, 1) < lax.broadcasted_iota(jnp.int32, square, 0)
    ).astype(f32)
    second = group.astype(f32)
    before_second = jnp.dot(
        earlier, jnp.broadcast_to(second, (seq, LANES)), preferred_element_type=f32
    )[:, 0:1]
    order = lax.broadcasted_iota(jnp.int32, (seq, 1), 0).astype(f32)
    place = jnp.where(second > 0.5, before_second + slots, order - before_second)
    spread = (
        place == lax.broadcasted_iota(jnp.int32, (seq, 2 * slots), 1).astype(f32)
    ).astype(bf16)

    def wait_mixed(k):
        of = lax.rem(me + k, n)
        mixed_copy(of, of).wait_recv()

    loop(1, n, wait_mixed)
    for d in range(n):
        columns = slice(d * depth, (d + 1) * depth)
        resid_rows[:, columns] = tokens[:, columns].astype(f32) + mixed[
            d, pl.ds(0, seq), :
        ].astype(f32)
    resid = resid_rows[...]
    moe_in = rms_normed(resid, moe_gain[...]).astype(bf16)
    first = (((0,), (0,)), ((), ()))
    for g in range(2):
        mine = spread[:, g * slots : (g + 1) * slots]
        packed[g, :, :model] = lax.dot_general(
            mine, moe_in, first, preferred_element_type=f32
        ).astype(bf16)
        packed[g, :, model:] = lax.dot_general(
            mine, shares, first, preferred_element_type=f32
        ).astype(bf16)

    half_chips = chips // 2

    def route_copy(j, slot):
        return remote(
            packed.at[j // half_chips],
            routed.at[2 * slot + core],
            send_f.at[j],
            recv_f.at[slot],
            2 * j + core,
        )

    def relay_copy(slot, side):
        return remote(
            routed.at[2 * slot + side],
            routed.at[2 * slot + side],
            send_g.at[slot],
            recv_g.at[slot],
            partner,
        )

    loop(1, chips, lambda k: route_copy(lax.rem(chip + k, chips), chip).start())
    routed[me] = packed[chip // half_chips]
    relay_copy(chip, core).start()

    def relay(k):
        slot = lax.rem(chip + chips - k, chips)
        route_copy(slot, slot).wait_recv()
        relay_copy(slot, core).start()

    loop(1, chips, relay)
    for load in loads[6:]:
        load.wait()
    loop(0, chips, lambda slot: relay_copy(slot, 1 - core).wait_recv())

    arrived = routed[...].reshape(n * slots, model + LANES)
    rows = arrived[:, :model]
    gate = jnp.dot(rows, gate_e[0], preferred_element_type=f32)
    upward = jnp.dot(rows, up_e[0], preferred_element_type=f32)
    inner = (gate * jax.nn.sigmoid(gate) * upward).astype(bf16)
    spot = lax.rem(me, group_width)
    lane = lax.broadcasted_iota(jnp.int32, (n * slots, LANES), 1)
    share = jnp.sum(
        jnp.where(
            (lane == spot) | (lane == spot + HALF), arrived[:, model:].astype(f32), 0.0
        ),
        axis=1,
        keepdims=True,
    )
    result = jnp.dot(inner, down_e[0], preferred_element_type=f32).astype(bf16).astype(f32)
    outcome[...] = (result * share).reshape(n, slots, model)

    def back_pair(j):
        return remote(
            back_pair_send.at[j], back_pair_recv.at[j], send_h.at[j], recv_h.at[j], partner
        )

    def send_back_pair(k):
        j = lax.rem(chip + k, chips)
        back_pair_send[j] = outcome[2 * j + 1 - core].astype(bf16)
        back_pair(j).start()

    loop(1, chips + 1, send_back_pair)

    def back_copy(j, slot):
        return remote(
            back_send.at[j], back_recv.at[slot], send_i.at[j], recv_i.at[slot], 2 * j + core
        )

    def send_back(k):
        j = lax.rem(chip + k, chips)
        back_pair(j).wait()
        back_send[j] = (outcome[2 * j + core] + back_pair_recv[j].astype(f32)).astype(bf16)
        back_copy(j, chip).start()

    loop(1, chips, send_back)
    back_pair(chip).wait()
    back_recv[chip] = (outcome[me] + back_pair_recv[chip].astype(f32)).astype(bf16)

    def wait_back(k):
        j = lax.rem(chip + k, chips)
        back_copy(j, j).wait()

    loop(1, chips, wait_back)
    combined = resid
    for g in range(2):
        base = g * half_chips
        total = lax.fori_loop(
            1,
            half_chips,
            lambda j, carry: carry + back_recv[base + j].astype(f32),
            back_recv[base].astype(f32),
        )
        high = total.astype(bf16)
        low = (total - high.astype(f32)).astype(bf16)
        mine = spread[:, g * slots : (g + 1) * slots]
        combined = combined + jnp.dot(mine, high, preferred_element_type=f32)
        combined = combined + jnp.dot(mine, low, preferred_element_type=f32)
    layer_out[...] = combined.astype(bf16)

    def sent(k):
        to = lax.rem(me + k, n)
        cell_copy(to, me).wait_send()
        mixed_copy(to, me).wait_send()

    loop(1, n, sent)
    loop(1, chips, lambda k: route_copy(lax.rem(chip + k, chips), chip).wait_send())
    loop(0, chips, lambda slot: relay_copy(slot, core).wait_send())
    memory_store.wait()


def on_device(
    tokens,
    norm_gain,
    query_weight,
    key_weight,
    value_weight,
    outgate_weight,
    ingate_weight,
    forget_weight,
    ingate_bias,
    forget_bias,
    memory,
    normalizer,
    stabilizer,
    mixer_weight,
    moe_gain,
    expert_gate,
    expert_up,
    expert_down,
    expert_index,
    route_weights,
):
    n = lax.axis_size("ep")
    seq, model = tokens.shape
    depth, width = query_weight.shape
    heads = ingate_bias.shape[0]
    hidden = expert_gate.shape[2]
    chosen_k = expert_index.shape[1]
    group_width = n // 2
    capacity = max(2, ((seq + 1) // 2 * chosen_k + group_width - 1) // group_width)
    most = min(seq, group_width * capacity // chosen_k)
    slots = (most + 7) // 8 * 8
    chips = n // 2
    total = 4 * width + LANES
    vmem = pl.BlockSpec(memory_space=pltpu.VMEM)
    hbm = pl.BlockSpec(memory_space=pl.ANY)
    dma = pltpu.SemaphoreType.DMA
    V = pltpu.VMEM
    wide, narrow = (n,), (chips,)
    return_shapes = (
        jax.ShapeDtypeStruct((seq, model), bf16),
        jax.ShapeDtypeStruct(normalizer.shape, f32),
        jax.ShapeDtypeStruct(stabilizer.shape, f32),
        jax.ShapeDtypeStruct(memory.shape, f32),
    )
    out, norm_out, stab_out, mem_out = pl.pallas_call(
        functools.partial(layer_kernel, n, seq, group_width),
        out_shape=return_shapes,
        in_specs=[vmem] * 11 + [hbm] * 9,
        out_specs=(vmem, vmem, vmem, hbm),
        scratch_shapes=[
            V((depth, 4 * width), bf16),
            V((depth, LANES), bf16),
            V(memory.shape, f32),
            V(mixer_weight.shape, bf16),
            V(expert_gate.shape, bf16),
            V(expert_up.shape, bf16),
            V(expert_down.shape, bf16),
            V((n, 16, depth), bf16),
            V((n, 16, depth), bf16),
            V((n, 16, total), f32),
            V((chips, 16, total), bf16),
            V((chips, 16, total), bf16),
            V((chips, 16, total), bf16),
            V((chips, 16, total), bf16),
            V((heads, M_HEAD_DIM, seq), f32),
            V((heads, M_HEAD_DIM, seq), f32),
            V((heads, seq, M_HEAD_DIM), f32),
            V((heads, seq, M_HEAD_DIM), f32),
            V((heads, seq, M_HEAD_DIM), f32),
            V((n, 16, width), bf16),
            V((n, 16, depth), bf16),
            V((n, 16, depth), bf16),
            V((seq, model), f32),
            V((2, slots, model + LANES), bf16),
            V((n, slots, model + LANES), bf16),
            V((n, slots, model), f32),
            V((chips, slots, model), bf16),
            V((chips, slots, model), bf16),
            V((chips, slots, model), bf16),
            V((chips, slots, model), bf16),
            dma((9,)),
            dma((1,)),
        ]
        + [dma(wide), dma(wide)]
        + [dma(narrow), dma(narrow)] * 2
        + [dma(wide), dma(wide)] * 2
        + [dma(narrow), dma(narrow)] * 4,
        compiler_params=pltpu.CompilerParams(
            collective_id=0, has_side_effects=True, vmem_limit_bytes=60 * 1024 * 1024
        ),
    )(
        tokens,
        norm_gain.reshape(1, model),
        ingate_weight,
        forget_weight,
        ingate_bias.reshape(1, heads),
        forget_bias.reshape(1, heads),
        normalizer,
        stabilizer,
        moe_gain.reshape(1, model),
        expert_index,
        route_weights,
        query_weight,
        key_weight,
        value_weight,
        outgate_weight,
        memory,
        mixer_weight,
        expert_gate,
        expert_up,
        expert_down,
    )
    return (out, mem_out, norm_out, stab_out)


def solution(mesh):
    return jax.shard_map(
        on_device,
        mesh=mesh,
        in_specs=(
            P(("grp", "ep"), None),
            P(),
            P("ep", None),
            P("ep", None),
            P("ep", None),
            P("ep", None),
            P("ep", None),
            P("ep", None),
            P(),
            P(),
            P(("grp", "ep"), None, None, None),
            P(("grp", "ep"), None, None),
            P(("grp", "ep"), None),
            P(None, "ep"),
            P(),
            P("ep", None, None),
            P("ep", None, None),
            P("ep", None, None),
            P(("grp", "ep"), None),
            P(("grp", "ep"), None),
        ),
        out_specs=(
            P(("grp", "ep"), None),
            P(("grp", "ep"), None, None, None),
            P(("grp", "ep"), None, None),
            P(("grp", "ep"), None),
        ),
        check_vma=False,
    )
```

time: 215 us -> 74.9 us (0.35)
  waiting for transfers between devices: 117 us -> 0 us
  Pallas kernels: 0 us -> 59.7 us
  blocking collectives: 36.9 us -> 0 us
  starting transfers between devices: 15.1 us -> 0 us
  between operations: 15.1 us -> 0.64 us
  other arithmetic: 9.43 us -> 0 us
  matrix products: 9.42 us -> 0 us
  local copies, waits for them, and re-layouts: 11.4 us -> 14.2 us
    unnamed x2 -> x0, waiting for transfers between devices: 92.5 us -> none
    pallas_call x0 -> x1, Pallas kernels: none -> 59.7 us  [on_device(): pl.pallas_call(functools.partial(layer_kernel, n, seq, group_width), out_...]
    all_to_all x3 -> x0, waiting for transfers between devices: 24.3 us -> none  [the longest x1 13.4 us: on_device(): lax.all_to_all(result, 'ep', split_axis=0, concat_axis=0, tiled=True)]
    all_gather x1 -> x0, blocking collectives: 20 us -> none  [on_device(): lax.all_gather(cell_out, 'ep', axis=0, tiled=True)]
    all_to_all x1 -> x0, blocking collectives: 16.9 us -> none  [on_device(): lax.all_to_all(outgoing, 'ep', split_axis=0, concat_axis=0, tiled=True)]
    all_to_all x3 -> x0, starting transfers between devices: 15 us -> none  [the longest x1 7.41 us: on_device(): lax.all_to_all(normed, 'ep', split_axis=1, concat_axis=0, tiled=True)]
    dot_general x7 -> x0, matrix products: 9.42 us -> none  [the longest x1 2.56 us: on_device(): jnp.einsum('sxcf,xfd->sxcd', inner, expert_down, preferred_element_type=f32)]
    unnamed x39 -> x11, local copies, waits for them, and re-layouts: 5.48 us -> 14.2 us
  transfers between devices with their start and end apart: 4 -> 0, of which waited for: 4 -> 0; matrix products, arithmetic and copies ran while one was open for 2% -> 0% of each run, Pallas kernels for 0% -> 0%
where the time goes in v1:
time: 74.9 us; the launch traced here: 74.6 us
  Pallas kernels  59.7 us (80%)
  local copies, waits for them, and re-layouts  14.2 us (19%)
    pallas_call x1, Pallas kernels, on_device(): pl.pallas_call(functools.partial(layer_kernel, n, seq, group_width), out_...  59.7 us
    unnamed x11, local copies, waits for them, and re-layouts  14.2 us

profile of v1, /device:TPU:0, one launch (start us, length us, event | category | flops | bytes accessed | tf_op | source)
XLA Modules:
  0.0 74.6 jit_solution(3424317335885238368)
XLA Ops:
  0.6 1.4 %copy.26.stabilizer = f32[12,4]{1,0:T(8,128)} copy(f32[12,4]{0,1:T(4,128)} %param.32) | data formatting | bytes 384 | tf_op args[12]
  2.0 1.4 %copy.27.expert_index = s32[12,6]{1,0:T(8,128)} copy(s32[12,6]{0,1:T(8,128)} %param.38) | data formatting | bytes 576 | tf_op args[18]
  3.4 1.4 %copy.28.route_weights = f32[12,6]{1,0:T(8,128)} copy(f32[12,6]{0,1:T(8,128)} %param.39) | data formatting | bytes 576 | tf_op args[19]
  4.7 1.4 %copy.24.ingate_weight = bf16[128,4]{1,0:T(8,128)(2,1)} copy(bf16[128,4]{0,1:T(4,128)(2,1)} %param.26) | data formatting | bytes 2048 | tf_op args[6]
  6.1 1.4 %copy.25.forget_weight = bf16[128,4]{1,0:T(8,128)(2,1)} copy(bf16[128,4]{0,1:T(4,128)(2,1)} %param.27) | data formatting | bytes 2048 | tf_op args[7]
  7.5 59.7 %shard_map.219 = (bf16[12,2048]{1,0:T(8,128)(2,1)}, f32[12,4,128]{2,1,0:T(4,128)}, f32[12,4]{1,0:T(8,128)}, f32[12,4,128,128]{3,2,1,0:T(8,128)}) custom-call(bf16[12,2048]{1,0:T(8,128)(2,1)} %tokens.1, f32[1,2048]{1,0:T(1,128)} %bitcast.4, bf16[128,4]{1,0:T(8,128)(2,1)} %copy.24.ingate_weight, bf16[128,4]{1,0:T(8,128)(2,1)} %copy.25.forget_weight, ...), custom_call_target="tpu_custom_call" | custom-call | tf_op jit(solution)/shard_map/pallas_call | solution.py:531
  67.2 1.4 %copy.29 = f32[12,4]{0,1:T(4,128)} copy(f32[12,4]{1,0:T(8,128)} %get-tuple-element.15) | data formatting | bytes 384
  68.6 1.5 %copy.33 = bf16[12,2048]{1,0:T(8,128)(2,1)} copy(bf16[12,2048]{1,0:T(8,128)(2,1)} %get-tuple-element.20) | data formatting | bytes 98304
  70.0 0.0 copy-start
  70.0 3.9 %copy.34 = f32[12,4,128,128]{3,2,1,0:T(8,128)} copy(f32[12,4,128,128]{3,2,1,0:T(8,128)} %get-tuple-element.21) | data formatting | bytes 6291456
  74.0 0.0 copy-done
  74.0 0.6 copy.35
Async XLA Ops:
  70.0 3.9 %copy-start = (f32[12,4,128]{2,1,0:T(4,128)S(1)}, f32[12,4,128]{2,1,0:T(4,128)}, u32[]{:S(2)}) copy-start(f32[12,4,128]{2,1,0:T(4,128)} %get-tuple-element.22) | copy-start | bytes 73732

commit v2 on v1

--- a/solution.py
+++ b/solution.py
@@ -73,6 +73,8 @@
     new_normalizer,
     new_stabilizer,
     new_memory,
+    small,
+    flip,
     proj_w,
     gate_w,
     mem,
@@ -113,6 +115,8 @@
     recv_c,
     send_d,
     recv_d,
+    relay_send,
+    relay_recv,
     send_e,
     recv_e,
     send_f,
@@ -133,6 +137,7 @@
     heads = mem.shape[1]
     model = tokens.shape[1]
     slots = packed.shape[1]
+    total = part.shape[2]
 
     loads = [
         pltpu.make_async_copy(source, target, load_sem.at[index])
@@ -171,10 +176,19 @@
     normed[:, pl.ds(seq, 16 - seq), :] = jnp.zeros((n, 16 - seq, depth), bf16)
     for d in range(n):
         normed[d, pl.ds(0, seq), :] = scaled[:, d * depth : (d + 1) * depth]
-    gate_w[...] = jnp.zeros(gate_w.shape, bf16)
+    gate_w[...] = jnp.zeros(gate_w.shape, f32)
     for base in (0, HALF):
-        gate_w[:, base : base + heads] = ingate_weight[...]
-        gate_w[:, base + heads : base + 2 * heads] = forget_weight[...]
+        gate_w[base : base + heads, :] = ingate_weight[...].astype(f32)
+        gate_w[base + heads : base + 2 * heads, :] = forget_weight[...].astype(f32)
+    top = expert_index.shape[0]
+    small[...] = jnp.zeros(small.shape, f32)
+    small[0:heads, 0:seq] = stabilizer[...]
+    small[8 : 8 + top, 0:seq] = route_weights[...]
+    small[16 : 16 + top, 0:seq] = expert_index[...].astype(f32)
+    flipped = small[...].T
+    old_stable = flipped[:seq, 0:heads]
+    route_share = flipped[:seq, 8 : 8 + top]
+    index = flipped[:seq, 16 : 16 + top]
 
     pl.semaphore_wait(barrier, n - 1)
 
@@ -197,7 +211,10 @@
         columns = slice(piece * width, (piece + 1) * width)
         block = jnp.dot(rows, proj_w[:, columns], preferred_element_type=f32)
         part[:, :, columns] = block.reshape(n, 16, width)
-    gates = jnp.dot(rows, gate_w[...], preferred_element_type=f32)
+    contract = (((1,), (1,)), ((), ()))
+    gates = lax.dot_general(
+        rows, gate_w[...].astype(bf16), contract, preferred_element_type=f32
+    )
     part[:, :, 4 * width :] = gates.reshape(n, 16, LANES)
 
     def pack_sums(values):
@@ -207,6 +224,23 @@
         narrow = values[:, 4 * width :]
         whole = narrow + pltpu.roll(narrow, HALF, 1)
         return jnp.concatenate([values[:, : 4 * width], whole], axis=1)
+
+    tail = sum_send.shape[2] - part.shape[2]
+
+    def fold(values):
+        rest = values[8:16]
+        moved = pltpu.roll(rest[:, tail:], 4, 0)
+        rest = jnp.concatenate(
+            [rest[:, : total - tail] + moved, rest[:, total - tail : tail]], axis=1
+        )
+        return values[:8], rest
+
+    def unfold(values):
+        rest = values[:, total:]
+        moved = pltpu.roll(rest[:, : total - tail], 4, 0)
+        return jnp.concatenate(
+            [values[:, :total], jnp.concatenate([rest, moved], axis=1)], axis=0
+        )
 
     def pair_copy(j):
         return remote(
@@ -235,36 +269,39 @@
         j = lax.rem(chip + k, chips)
         pair_copy(j).wait()
         wide, narrow = pack_sums(part[2 * j + core] + unpack_sums(pair_recv[j].astype(f32)))
-        sum_send[j, :, : 4 * width] = wide
-        sum_send[j, :, 4 * width :] = narrow
+        joined = jnp.concatenate([wide.astype(f32), narrow.astype(f32)], axis=1)
+        head, rest = fold(joined)
+        sum_send[j, :, :total] = head.astype(bf16)
+        sum_send[j, :, total:] = rest.astype(bf16)
         sum_copy(j, chip).start()
 
     loop(1, chips, send_sum)
     pair_copy(chip).wait()
     own = part[me] + unpack_sums(pair_recv[chip].astype(f32))
 
-    def wait_sum(k, total):
+    def wait_sum(k, carry):
         j = lax.rem(chip + k, chips)
         sum_copy(j, j).wait()
-        return total + sum_recv[j].astype(f32)
-
-    others = lax.fori_loop(1, chips, wait_sum, jnp.zeros(own.shape, f32))
-    sums = (own + unpack_sums(others))[:seq]
+        return carry + sum_recv[j].astype(f32)
+
+    others = lax.fori_loop(1, chips, wait_sum, jnp.zeros(sum_recv.shape[1:], f32))
+    sums = (own + unpack_sums(unfold(others)))[:seq]
 
     scale = M_HEAD_DIM ** (-0.5)
     gates = sums[:, 4 * width : 4 * width + 2 * heads]
     ingate_pre = gates[:, :heads] + ingate_bias[...]
     forget_pre = gates[:, heads:] + forget_bias[...]
     log_forget = jnp.minimum(forget_pre, 0.0) - jnp.log1p(jnp.exp(-jnp.abs(forget_pre)))
-    stable = jnp.maximum(log_forget + stabilizer[...], ingate_pre)
-    new_stabilizer[...] = stable
-    keep = jnp.exp(log_forget + stabilizer[...] - stable)
+    stable = jnp.maximum(log_forget + old_stable, ingate_pre)
+    flip[...] = jnp.zeros(flip.shape, f32)
+    flip[0:seq, 0:heads] = stable
+    new_stabilizer[...] = flip[...].T[:heads, :seq]
+    keep = jnp.exp(log_forget + old_stable - stable)
     write = jnp.exp(ingate_pre - stable)
     rank = (M_HEAD_DIM, M_HEAD_DIM)
     unit = (
         lax.broadcasted_iota(jnp.int32, rank, 0) == lax.broadcasted_iota(jnp.int32, rank, 1)
     ).astype(bf16)
-    contract = (((1,), (1,)), ((), ()))
     denoms = []
     for h in range(heads):
         lanes = slice(h * M_HEAD_DIM, (h + 1) * M_HEAD_DIM)
@@ -305,17 +342,25 @@
         hidden = numer[h] / jnp.maximum(jnp.abs(denoms[h]), 1.0)
         cells[me, pl.ds(0, seq), lanes] = (hidden * opened[:, lanes]).astype(bf16)
 
-    def cell_copy(to, slot):
-        return remote(cells.at[slot], cells.at[slot], send_d.at[to], recv_d.at[slot], to)
-
-    loop(1, n, lambda k: cell_copy(lax.rem(me + k, n), me).start())
+    def cell_copy(j, slot):
+        own = cells.at[2 * slot + core]
+        return remote(own, own, send_d.at[j], recv_d.at[slot], 2 * j + core)
+
+    def cell_relay(slot, side):
+        own = cells.at[2 * slot + side]
+        return remote(own, own, relay_send.at[slot], relay_recv.at[slot], partner)
+
+    loop(1, chips, lambda k: cell_copy(lax.rem(chip + k, chips), chip).start())
+    cell_relay(chip, core).start()
     loads[5].wait()
 
-    def wait_cell(k):
-        of = lax.rem(me + k, n)
-        cell_copy(of, of).wait_recv()
-
-    loop(1, n, wait_cell)
+    def relay_cell(k):
+        slot = lax.rem(chip + chips - k, chips)
+        cell_copy(slot, slot).wait_recv()
+        cell_relay(slot, core).start()
+
+    loop(1, chips, relay_cell)
+    loop(0, chips, lambda slot: cell_relay(slot, 1 - core).wait_recv())
     mixes = jnp.dot(
         cells[...].reshape(n * 16, width), mix_w[...], preferred_element_type=f32
     ).astype(bf16)
@@ -327,15 +372,14 @@
     loop(1, n, lambda k: mixed_copy(lax.rem(me + k, n), me).start())
     mixed[me] = mixed_send[me]
 
-    index = expert_index[...]
     group = (index[:, 0:1] >= group_width).astype(jnp.int32)
     lane = lax.broadcasted_iota(jnp.int32, (seq, LANES), 1)
     named = group * group_width + jnp.where(lane < HALF, lane, lane - HALF)
     inside = jnp.where(lane < HALF, lane, lane - HALF) < group_width
     shares = jnp.zeros((seq, LANES), f32)
-    for k in range(index.shape[1]):
-        hit = (index[:, k : k + 1] == named) & inside
-        shares = shares + jnp.where(hit, route_weights[:, k : k + 1], 0.0)
+    for k in range(top):
+        hit = (index[:, k : k + 1] == named.astype(f32)) & inside
+        shares = shares + jnp.where(hit, route_share[:, k : k + 1], 0.0)
     shares = split_lanes(shares)
     square = (seq, seq)
     earlier = (
@@ -459,14 +503,14 @@
     combined = resid
     for g in range(2):
         base = g * half_chips
-        total = lax.fori_loop(
+        back = lax.fori_loop(
             1,
             half_chips,
             lambda j, carry: carry + back_recv[base + j].astype(f32),
             back_recv[base].astype(f32),
         )
-        high = total.astype(bf16)
-        low = (total - high.astype(f32)).astype(bf16)
+        high = back.astype(bf16)
+        low = (back - high.astype(f32)).astype(bf16)
         mine = spread[:, g * slots : (g + 1) * slots]
         combined = combined + jnp.dot(mine, high, preferred_element_type=f32)
         combined = combined + jnp.dot(mine, low, preferred_element_type=f32)
@@ -474,10 +518,11 @@
 
     def sent(k):
         to = lax.rem(me + k, n)
-        cell_copy(to, me).wait_send()
         mixed_copy(to, me).wait_send()
 
     loop(1, n, sent)
+    loop(1, chips, lambda k: cell_copy(lax.rem(chip + k, chips), chip).wait_send())
+    loop(0, chips, lambda slot: cell_relay(slot, core).wait_send())
     loop(1, chips, lambda k: route_copy(lax.rem(chip + k, chips), chip).wait_send())
     loop(0, chips, lambda slot: relay_copy(slot, core).wait_send())
     memory_store.wait()
@@ -517,6 +562,8 @@
     slots = (most + 7) // 8 * 8
     chips = n // 2
     total = 4 * width + LANES
+    tail = (total // LANES + 1) // 2 * LANES
+    assert 8 < seq <= 12
     vmem = pl.BlockSpec(memory_space=pltpu.VMEM)
     hbm = pl.BlockSpec(memory_space=pl.ANY)
     dma = pltpu.SemaphoreType.DMA
@@ -525,7 +572,7 @@
     return_shapes = (
         jax.ShapeDtypeStruct((seq, model), bf16),
         jax.ShapeDtypeStruct(normalizer.shape, f32),
-        jax.ShapeDtypeStruct(stabilizer.shape, f32),
+        jax.ShapeDtypeStruct((heads, seq), f32),
         jax.ShapeDtypeStruct(memory.shape, f32),
     )
     out, norm_out, stab_out, mem_out = pl.pallas_call(
@@ -534,8 +581,10 @@
         in_specs=[vmem] * 11 + [hbm] * 9,
         out_specs=(vmem, vmem, vmem, hbm),
         scratch_shapes=[
+            V((32, LANES), f32),
+            V((16, LANES), f32),
             V((depth, 4 * width), bf16),
-            V((depth, LANES), bf16),
+            V((LANES, depth), f32),
             V(memory.shape, f32),
             V(mixer_weight.shape, bf16),
             V(expert_gate.shape, bf16),
@@ -546,8 +595,8 @@
             V((n, 16, total), f32),
             V((chips, 16, total), bf16),
             V((chips, 16, total), bf16),
-            V((chips, 16, total), bf16),
-            V((chips, 16, total), bf16),
+            V((chips, 8, total + tail), bf16),
+            V((chips, 8, total + tail), bf16),
             V((heads, M_HEAD_DIM, seq), f32),
             V((heads, M_HEAD_DIM, seq), f32),
             V((heads, seq, M_HEAD_DIM), f32),
@@ -568,8 +617,8 @@
             dma((1,)),
         ]
         + [dma(wide), dma(wide)]
-        + [dma(narrow), dma(narrow)] * 2
-        + [dma(wide), dma(wide)] * 2
+        + [dma(narrow), dma(narrow)] * 4
+        + [dma(wide), dma(wide)]
         + [dma(narrow), dma(narrow)] * 4,
         compiler_params=pltpu.CompilerParams(
             collective_id=0, has_side_effects=True, vmem_limit_bytes=60 * 1024 * 1024
@@ -577,15 +626,15 @@
     )(
         tokens,
         norm_gain.reshape(1, model),
-        ingate_weight,
-        forget_weight,
+        ingate_weight.T,
+        forget_weight.T,
         ingate_bias.reshape(1, heads),
         forget_bias.reshape(1, heads),
         normalizer,
-        stabilizer,
+        stabilizer.T,
         moe_gain.reshape(1, model),
-        expert_index,
-        route_weights,
+        expert_index.T,
+        route_weights.T,
         query_weight,
         key_weight,
         value_weight,
@@ -596,7 +645,7 @@
         expert_up,
         expert_down,
     )
-    return (out, mem_out, norm_out, stab_out)
+    return (out, mem_out, norm_out, stab_out.T)
 
 
 def solution(mesh):

time: 74.9 us -> 62.9 us (0.84)
  local copies, waits for them, and re-layouts: 14.2 us -> 6.58 us
  Pallas kernels: 59.7 us -> 55.4 us
    unnamed x11 -> x8, local copies, waits for them, and re-layouts: 14.2 us -> 6.58 us
    pallas_call x1, Pallas kernels: 59.7 us -> 55.4 us  [on_device(): pl.pallas_call(functools.partial(layer_kernel, n, seq, group_width), out_...]
where the time goes in v2:
time: 62.9 us; the launch traced here: 62.6 us
  Pallas kernels  55.4 us (88%)
  local copies, waits for them, and re-layouts  6.58 us (10%)
  between operations  0.65 us (1%)
    pallas_call x1, Pallas kernels, on_device(): pl.pallas_call(functools.partial(layer_kernel, n, seq, group_width), out_...  55.4 us
    unnamed x8, local copies, waits for them, and re-layouts  6.58 us

profile of v2, /device:TPU:0, one launch (start us, length us, event | category | flops | bytes accessed | tf_op | source)
XLA Modules:
  0.0 62.6 jit_solution(10597775918595858431)
XLA Ops:
  0.6 55.4 %shard_map.219 = (bf16[12,2048]{1,0:T(8,128)(2,1)}, f32[12,4,128]{2,1,0:T(4,128)}, f32[4,12]{1,0:T(4,128)}, f32[12,4,128,128]{3,2,1,0:T(8,128)}) custom-call(bf16[12,2048]{1,0:T(8,128)(2,1)} %tokens.1, f32[1,2048]{1,0:T(1,128)} %bitcast.10, bf16[4,128]{1,0:T(4,128)(2,1)} %bitcast.16, bf16[4,128]{1,0:T(4,128)(2,1)} %bitcast.17, f32[1,4]{1,0:T(1,128)} %bitcast.18, ...), custom_call_target="tpu_custom_call" | custom-call | tf_op jit(solution)/shard_map/pallas_call | solution.py:578
  56.0 1.5 %copy.28 = bf16[12,2048]{1,0:T(8,128)(2,1)} copy(bf16[12,2048]{1,0:T(8,128)(2,1)} %get-tuple-element.16) | data formatting | bytes 98304
  57.5 0.0 copy-start
  57.5 0.0 copy-start.1
  57.5 3.9 %copy.29 = f32[12,4,128,128]{3,2,1,0:T(8,128)} copy(f32[12,4,128,128]{3,2,1,0:T(8,128)} %get-tuple-element.17) | data formatting | bytes 6291456
  61.4 0.0 copy-done
  61.4 0.6 copy.30
  62.1 0.0 copy-done.1
  62.1 0.6 copy.31
Async XLA Ops:
  57.5 3.9 %copy-start = (f32[12,4,128]{2,1,0:T(4,128)S(1)}, f32[12,4,128]{2,1,0:T(4,128)}, u32[]{:S(2)}) copy-start(f32[12,4,128]{2,1,0:T(4,128)} %get-tuple-element.18) | copy-start | bytes 73732
  57.5 4.5 %copy-start.1 = (f32[4,12]{1,0:T(4,128)S(1)}, f32[4,12]{1,0:T(4,128)}, u32[]{:S(2)}) copy-start(f32[4,12]{1,0:T(4,128)} %get-tuple-element.11) | copy-start | bytes 580

commit v3 on v2

--- a/solution.py
+++ b/solution.py
@@ -37,6 +37,11 @@
         return carry
 
     lax.fori_loop(low, high, step, 0)
+
+
+def far_first(k, count):
+    half = count // 2
+    return half + (1 - 2 * lax.rem(k, 2)) * (k // 2)
 
 
 def split_lanes(values):
@@ -106,7 +111,6 @@
     back_send,
     back_recv,
     load_sem,
-    store_sem,
     send_a,
     recv_a,
     send_b,
@@ -164,7 +168,7 @@
         pl.semaphore_signal(
             barrier,
             inc=1,
-            device_id={"ep": lax.rem(me + k, n)},
+            device_id={"ep": lax.rem(me + far_first(k, n), n)},
             device_id_type=pl.DeviceIdType.MESH,
         )
 
@@ -193,11 +197,11 @@
     pl.semaphore_wait(barrier, n - 1)
 
     def send_cols(k):
-        to = lax.rem(me + k, n)
+        to = lax.rem(me + far_first(k, n), n)
         remote(normed.at[to], normed_cols.at[me], send_a.at[to], recv_a.at[me], to).start()
 
     def wait_cols(k):
-        of = lax.rem(me + k, n)
+        of = lax.rem(me + far_first(k, n), n)
         remote(normed.at[of], normed_cols.at[of], send_a.at[of], recv_a.at[of], of).wait()
 
     loop(1, n, send_cols)
@@ -248,13 +252,16 @@
         )
 
     def send_pair(k):
-        j = lax.rem(chip + k, chips)
+        send_pair_of(lax.rem(chip + far_first(k, chips), chips))
+
+    def send_pair_of(j):
         wide, narrow = pack_sums(part[2 * j + 1 - core])
         pair_send[j, :, : 4 * width] = wide
         pair_send[j, :, 4 * width :] = narrow
         pair_copy(j).start()
 
-    loop(1, chips + 1, send_pair)
+    loop(1, chips, send_pair)
+    send_pair_of(chip)
 
     def sum_copy(j, slot):
         return remote(
@@ -266,7 +273,7 @@
         )
 
     def send_sum(k):
-        j = lax.rem(chip + k, chips)
+        j = lax.rem(chip + far_first(k, chips), chips)
         pair_copy(j).wait()
         wide, narrow = pack_sums(part[2 * j + core] + unpack_sums(pair_recv[j].astype(f32)))
         joined = jnp.concatenate([wide.astype(f32), narrow.astype(f32)], axis=1)
@@ -280,7 +287,7 @@
     own = part[me] + unpack_sums(pair_recv[chip].astype(f32))
 
     def wait_sum(k, carry):
-        j = lax.rem(chip + k, chips)
+        j = lax.rem(chip + far_first(k, chips), chips)
         sum_copy(j, j).wait()
         return carry + sum_recv[j].astype(f32)
 
@@ -326,14 +333,12 @@
                 keep_rows[h, t : t + 1, :] * mem[t, h]
                 + key_t[h, :, t : t + 1] * value_rows[h, t : t + 1, :]
             )
-            mem[t, h] = fresh
+            new_memory[t, h] = fresh
             numer[h, t : t + 1, :] = jnp.sum(
                 query_t[h, :, t : t + 1] * fresh, axis=0, keepdims=True
             )
 
     loop(0, heads, one_head)
-    memory_store = pltpu.make_async_copy(mem, new_memory, store_sem.at[0])
-    memory_store.start()
     outgate = sums[:, 3 * width : 4 * width].astype(bf16).astype(f32)
     opened = jax.nn.sigmoid(outgate)
     cells[me] = jnp.zeros(cells.shape[1:], bf16)
@@ -350,12 +355,12 @@
         own = cells.at[2 * slot + side]
         return remote(own, own, relay_send.at[slot], relay_recv.at[slot], partner)
 
-    loop(1, chips, lambda k: cell_copy(lax.rem(chip + k, chips), chip).start())
+    loop(1, chips, lambda k: cell_copy(lax.rem(chip + far_first(k, chips), chips), chip).start())
     cell_relay(chip, core).start()
     loads[5].wait()
 
     def relay_cell(k):
-        slot = lax.rem(chip + chips - k, chips)
+        slot = lax.rem(chip + chips - far_first(k, chips), chips)
         cell_copy(slot, slot).wait_recv()
         cell_relay(slot, core).start()
 
@@ -369,7 +374,7 @@
     def mixed_copy(to, slot):
         return remote(mixed_send.at[to], mixed.at[slot], send_e.at[to], recv_e.at[slot], to)
 
-    loop(1, n, lambda k: mixed_copy(lax.rem(me + k, n), me).start())
+    loop(1, n, lambda k: mixed_copy(lax.rem(me + far_first(k, n), n), me).start())
     mixed[me] = mixed_send[me]
 
     group = (index[:, 0:1] >= group_width).astype(jnp.int32)
@@ -396,7 +401,7 @@
     ).astype(bf16)
 
     def wait_mixed(k):
-        of = lax.rem(me + k, n)
+        of = lax.rem(me + far_first(k, n), n)
         mixed_copy(of, of).wait_recv()
 
     loop(1, n, wait_mixed)
@@ -437,12 +442,12 @@
             partner,
         )
 
-    loop(1, chips, lambda k: route_copy(lax.rem(chip + k, chips), chip).start())
+    loop(1, chips, lambda k: route_copy(lax.rem(chip + far_first(k, chips), chips), chip).start())
     routed[me] = packed[chip // half_chips]
     relay_copy(chip, core).start()
 
     def relay(k):
-        slot = lax.rem(chip + chips - k, chips)
+        slot = lax.rem(chip + chips - far_first(k, chips), chips)
         route_copy(slot, slot).wait_recv()
         relay_copy(slot, core).start()
 
@@ -474,11 +479,14 @@
         )
 
     def send_back_pair(k):
-        j = lax.rem(chip + k, chips)
+        send_back_pair_of(lax.rem(chip + far_first(k, chips), chips))
+
+    def send_back_pair_of(j):
         back_pair_send[j] = outcome[2 * j + 1 - core].astype(bf16)
         back_pair(j).start()
 
-    loop(1, chips + 1, send_back_pair)
+    loop(1, chips, send_back_pair)
+    send_back_pair_of(chip)
 
     def back_copy(j, slot):
         return remote(
@@ -486,7 +494,7 @@
         )
 
     def send_back(k):
-        j = lax.rem(chip + k, chips)
+        j = lax.rem(chip + far_first(k, chips), chips)
         back_pair(j).wait()
         back_send[j] = (outcome[2 * j + core] + back_pair_recv[j].astype(f32)).astype(bf16)
         back_copy(j, chip).start()
@@ -496,7 +504,7 @@
     back_recv[chip] = (outcome[me] + back_pair_recv[chip].astype(f32)).astype(bf16)
 
     def wait_back(k):
-        j = lax.rem(chip + k, chips)
+        j = lax.rem(chip + far_first(k, chips), chips)
         back_copy(j, j).wait()
 
     loop(1, chips, wait_back)
@@ -517,15 +525,14 @@
     layer_out[...] = combined.astype(bf16)
 
     def sent(k):
-        to = lax.rem(me + k, n)
+        to = lax.rem(me + far_first(k, n), n)
         mixed_copy(to, me).wait_send()
 
     loop(1, n, sent)
-    loop(1, chips, lambda k: cell_copy(lax.rem(chip + k, chips), chip).wait_send())
+    loop(1, chips, lambda k: cell_copy(lax.rem(chip + far_first(k, chips), chips), chip).wait_send())
     loop(0, chips, lambda slot: cell_relay(slot, core).wait_send())
-    loop(1, chips, lambda k: route_copy(lax.rem(chip + k, chips), chip).wait_send())
+    loop(1, chips, lambda k: route_copy(lax.rem(chip + far_first(k, chips), chips), chip).wait_send())
     loop(0, chips, lambda slot: relay_copy(slot, core).wait_send())
-    memory_store.wait()
 
 
 def on_device(
@@ -565,21 +572,21 @@
     tail = (total // LANES + 1) // 2 * LANES
     assert 8 < seq <= 12
     vmem = pl.BlockSpec(memory_space=pltpu.VMEM)
-    hbm = pl.BlockSpec(memory_space=pl.ANY)
+    hbm = pl.BlockSpec(memory_space=pltpu.HBM)
     dma = pltpu.SemaphoreType.DMA
     V = pltpu.VMEM
     wide, narrow = (n,), (chips,)
     return_shapes = (
-        jax.ShapeDtypeStruct((seq, model), bf16),
-        jax.ShapeDtypeStruct(normalizer.shape, f32),
-        jax.ShapeDtypeStruct((heads, seq), f32),
-        jax.ShapeDtypeStruct(memory.shape, f32),
+        pltpu.VMEM((seq, model), bf16),
+        pltpu.VMEM(normalizer.shape, f32),
+        pltpu.VMEM((heads, seq), f32),
+        pltpu.VMEM(memory.shape, f32),
     )
     out, norm_out, stab_out, mem_out = pl.pallas_call(
         functools.partial(layer_kernel, n, seq, group_width),
         out_shape=return_shapes,
         in_specs=[vmem] * 11 + [hbm] * 9,
-        out_specs=(vmem, vmem, vmem, hbm),
+        out_specs=(vmem, vmem, vmem, vmem),
         scratch_shapes=[
             V((32, LANES), f32),
             V((16, LANES), f32),
@@ -614,14 +621,13 @@
             V((chips, slots, model), bf16),
             V((chips, slots, model), bf16),
             dma((9,)),
-            dma((1,)),
         ]
         + [dma(wide), dma(wide)]
         + [dma(narrow), dma(narrow)] * 4
         + [dma(wide), dma(wide)]
         + [dma(narrow), dma(narrow)] * 4,
         compiler_params=pltpu.CompilerParams(
-            collective_id=0, has_side_effects=True, vmem_limit_bytes=60 * 1024 * 1024
+            collective_id=0, has_side_effects=True, vmem_limit_bytes=54 * 1024 * 1024
         ),
     )(
         tokens,

time: 62.9 us -> 62 us (0.986)
  local copies, waits for them, and re-layouts: 6.58 us -> 3.48 us
  Pallas kernels: 55.4 us -> 57.7 us
    unnamed x8 -> x4, local copies, waits for them, and re-layouts: 6.58 us -> 3.48 us
    pallas_call x1, Pallas kernels: 55.4 us -> 57.7 us  [on_device(): pl.pallas_call(functools.partial(layer_kernel, n, seq, group_width), out_...]
where the time goes in v3:
time: 62 us; the launch traced here: 61.9 us
  Pallas kernels  57.7 us (93%)
  local copies, waits for them, and re-layouts  3.48 us (6%)
  between operations  0.65 us (1%)
    pallas_call x1, Pallas kernels, on_device(): pl.pallas_call(functools.partial(layer_kernel, n, seq, group_width), out_...  57.7 us
    unnamed x4, local copies, waits for them, and re-layouts  3.48 us

profile of v3, /device:TPU:0, one launch (start us, length us, event | category | flops | bytes accessed | tf_op | source)
XLA Modules:
  0.0 61.9 jit_solution(4837125190228902439)
XLA Ops:
  0.6 57.7 %shard_map.219 = (bf16[12,2048]{1,0:T(8,128)(2,1)S(1)}, f32[12,4,128]{2,1,0:T(4,128)S(1)}, f32[4,12]{1,0:T(4,128)S(1)}, f32[12,4,128,128]{3,2,1,0:T(8,128)S(1)}) custom-call(bf16[12,2048]{1,0:T(8,128)(2,1)} %tokens.1, f32[1,2048]{1,0:T(1,128)} %bitcast.11, bf16[4,128]{1,0:T(4,128)(2,1)} %bitcast.16, bf16[4,128]{1,0:T(4,128)(2,1)} %bitcast.17, ...), custom_call_target="tpu_custom_call" | custom-call | tf_op jit(solution)/shard_map/pallas_call | solution.py:585
  58.4 0.6 %copy.28 = bf16[12,2048]{1,0:T(8,128)(2,1)} copy(bf16[12,2048]{1,0:T(8,128)(2,1)S(1)} %get-tuple-element.12) | data formatting | bytes 98304
  59.0 0.6 copy.31
  59.6 0.6 copy.30
  60.2 1.7 %copy.29 = f32[12,4,128,128]{3,2,1,0:T(8,128)} copy(f32[12,4,128,128]{3,2,1,0:T(8,128)S(1)} %get-tuple-element.13) | data formatting | bytes 6291456
